TPU v7x, 32 devices: a whole 2x2x4 slice. The times are simulated.
32 devices in a mesh: kv: 8 (over z, y), tp: 4 (over x, core).
Axes of the slice: x: 2, y: 2, z: 4, core: 2. Of those that a mesh axis runs over, the one named last changes fastest.
Arguments:
- piece_tokens: bfloat16 [32, 2048], P('kv'), may hold values from -6 to 6
- decode_tokens: bfloat16 [8, 2048], P('kv'), may hold values from -6 to 6
- prompt_fill: int32 [1], replicated, may hold values from 1024 to 2016
- decode_fill: int32 [8], P('kv'), may hold values from 1 to 767, 3072 in all
- prompt_cache: bfloat16 [2048, 544], P('kv'), may hold values from -600 to 600
- decode_cache: bfloat16 [8, 768, 544], P('kv'), may hold values from -600 to 600
- input_gain: float32 [2048], replicated, may hold values from 0.1 to 1.9
- query_gain: float32 [768], replicated, may hold values from 0.1 to 1.9
- latent_gain: float32 [512], replicated, may hold values from 0.1 to 1.9
- query_down: bfloat16 [2048, 768], P(None, 'tp'), may hold values from -0.125 to 0.125
- latent_down: bfloat16 [2048, 512], P(None, 'tp'), may hold values from -0.125 to 0.125
- rope_down: bfloat16 [2048, 32], replicated, may hold values from -0.125 to 0.125
- query_up: bfloat16 [768, 1024], P(None, 'tp'), may hold values from -0.21875 to 0.21875
- qrope_up: bfloat16 [768, 512], P(None, 'tp'), may hold values from -0.21875 to 0.21875
- key_up: bfloat16 [16, 64, 512], P('tp'), may hold values from -0.25 to 0.25
- value_up: bfloat16 [16, 512, 64], P('tp'), may hold values from -4 to 4
- out_proj: bfloat16 [1024, 2048], P('tp'), may hold values from -4 to 4
Outputs:
- piece_out: bfloat16 [32, 2048], P('kv')
- decode_out: bfloat16 [8, 2048], P('kv')
- piece_rows: bfloat16 [32, 544], P('kv')
- decode_rows: bfloat16 [8, 544], P('kv')
Inputs may be any that keep to these rules, and one draw needn't show every extreme that they name: `prompt_fill`: the piece takes the 32 positions that follow the cache's filled positions. `decode_fill`: a decoding sequence's new token takes the position that follows its filled ones.
All inputs are finite; a program needn't handle non-finite values. No bound on the sum of `decode_fill` on one device may be relied on, other than what follows from the above.
Results may differ from a plain program's by a relative error of at most 0.035.
Values may be sent and summed in bfloat16 or wider, within the bound.
A program may use at most 64 MiB of HBM per device.

v0:
```python
import jax
import jax.numpy as jnp
from jax import lax
from jax.sharding import PartitionSpec as P

NOPE = 64
ROPE = 32
NEG_FILL = -1e30
RMS_EPS = 1e-06
THETA = 10000.0


def rms_scale(values, gain_row):
    widened = values.astype(jnp.float32)
    scaled = (
        widened
        * lax.rsqrt(jnp.mean(widened * widened, axis=-1, keepdims=True) + RMS_EPS)
        * gain_row
    )
    return scaled.astype(jnp.bfloat16)


def rotate(values, places):
    half_width = values.shape[-1] // 2
    inverse = THETA ** (-jnp.arange(half_width, dtype=jnp.float32) / half_width)
    angles = places.astype(jnp.float32)[..., None] * inverse
    first_half = values[..., :half_width].astype(jnp.float32)
    second_half = values[..., half_width:].astype(jnp.float32)
    cosine = jnp.cos(angles)
    sine_part = jnp.sin(angles)
    return jnp.concatenate(
        [
            first_half * cosine - second_half * sine_part,
            first_half * sine_part + second_half * cosine,
        ],
        axis=-1,
    ).astype(jnp.bfloat16)


def make_queries(query_lat, places, query_up, qrope_up, key_up):
    row_count = query_lat.shape[0]
    head_count = key_up.shape[0]
    nope_part = (
        jnp.dot(query_lat, query_up, preferred_element_type=jnp.float32)
        .astype(jnp.bfloat16)
        .reshape(row_count, head_count, -1)
    )
    rope_raw = (
        jnp.dot(query_lat, qrope_up, preferred_element_type=jnp.float32)
        .astype(jnp.bfloat16)
        .reshape(row_count, head_count, -1)
    )
    turned = rotate(rope_raw, places[:, None])
    absorbed = jnp.einsum(
        "nhc,hcl->nhl", nope_part, key_up, preferred_element_type=jnp.float32
    ).astype(jnp.bfloat16)
    return (absorbed, turned)


def block_attend(absorbed, turned, key_rows, key_places, query_places, value_up):
    latent_width = value_up.shape[1]
    score_scale = (NOPE + ROPE) ** (-0.5)
    latent_keys = key_rows[:, :latent_width]
    scores = (
        jnp.einsum("nhl,sl->nhs", absorbed, latent_keys, preferred_element_type=jnp.float32)
        + jnp.einsum(
            "nhr,sr->nhs", turned, key_rows[:, latent_width:], preferred_element_type=jnp.float32
        )
    ) * score_scale
    allowed = key_places[None, None, :] <= query_places[:, None, None]
    scores = jnp.where(allowed, scores, NEG_FILL)
    local_peak = jnp.max(scores, axis=-1)
    exp_scores = jnp.where(allowed, jnp.exp(scores - local_peak[..., None]), 0.0)
    weight_sum = jnp.sum(exp_scores, axis=-1)
    weights = exp_scores.astype(jnp.bfloat16)
    mixed_rows = jnp.einsum("nhs,sl->nhl", weights, latent_keys, preferred_element_type=jnp.float32)
    partial_sum = jnp.einsum(
        "nhl,hlv->nhv", mixed_rows, value_up.astype(jnp.float32), precision=lax.Precision.HIGHEST
    )
    return (partial_sum, weight_sum, local_peak)


def insert_row(cache_rows, new_row, fill_one):
    return lax.dynamic_update_slice(cache_rows, new_row[None], (fill_one, jnp.zeros((), jnp.int32)))


def local(
    piece_tokens,
    decode_tokens,
    prompt_fill,
    decode_fill,
    prompt_cache,
    decode_cache,
    input_gain,
    query_gain,
    latent_gain,
    query_down,
    latent_down,
    rope_down,
    query_up,
    qrope_up,
    key_up,
    value_up,
    out_proj,
):
    kv_index = lax.axis_index("kv")
    piece_dev = piece_tokens.shape[0]
    shard_len = prompt_cache.shape[0]
    fill_start = prompt_fill[0]
    own_places = fill_start + kv_index * piece_dev + jnp.arange(piece_dev, dtype=jnp.int32)
    places = jnp.concatenate([own_places, decode_fill])
    tokens = jnp.concatenate([piece_tokens, decode_tokens], axis=0)
    normed = rms_scale(tokens, input_gain)
    query_comp = jnp.dot(normed, query_down, preferred_element_type=jnp.float32).astype(
        jnp.bfloat16
    )
    latent_comp = jnp.dot(normed, latent_down, preferred_element_type=jnp.float32).astype(
        jnp.bfloat16
    )
    query_comp, latent_comp = (
        lax.all_gather(query_comp, "tp", axis=1, tiled=True),
        lax.all_gather(latent_comp, "tp", axis=1, tiled=True),
    )
    query_lat = rms_scale(query_comp, query_gain)
    rope_raw = jnp.dot(normed, rope_down, preferred_element_type=jnp.float32).astype(jnp.bfloat16)
    new_rows = jnp.concatenate(
        [rms_scale(latent_comp, latent_gain), rotate(rope_raw, places)], axis=-1
    )
    piece_rows = new_rows[:piece_dev]
    decode_rows = new_rows[piece_dev:]
    decode_absorbed, decode_turned = make_queries(
        query_lat[piece_dev:], decode_fill, query_up, qrope_up, key_up
    )
    piece_latent, arrived = (
        lax.all_gather(query_lat[:piece_dev], "kv", axis=0, tiled=True),
        lax.all_gather(piece_rows, "kv", axis=0, tiled=True),
    )
    arrived_places = fill_start + jnp.arange(arrived.shape[0], dtype=jnp.int32)
    piece_absorbed, piece_turned = make_queries(
        piece_latent, arrived_places, query_up, qrope_up, key_up
    )
    piece_total = arrived.shape[0]
    query_places = fill_start + jnp.arange(piece_total, dtype=jnp.int32)
    zero_rows = jnp.zeros((shard_len, arrived.shape[1]), arrived.dtype)
    padded = jnp.concatenate([zero_rows, arrived, zero_rows], axis=0)
    offset = jnp.clip(kv_index * shard_len - fill_start + shard_len, 0, piece_total + shard_len)
    window = lax.dynamic_slice_in_dim(padded, offset, shard_len, 0)
    key_places = kv_index * shard_len + jnp.arange(shard_len, dtype=jnp.int32)
    fresh_rows = (key_places >= fill_start) & (key_places < fill_start + piece_total)
    key_rows = jnp.where(fresh_rows[:, None], window, prompt_cache)
    partial_sum, weight_sum, local_peak = block_attend(
        piece_absorbed, piece_turned, key_rows, key_places, query_places, value_up
    )
    all_parts, all_totals, all_peaks = (
        lax.all_to_all(
            partial_sum.reshape(1, piece_total, -1), "kv", split_axis=1, concat_axis=0, tiled=True
        ),
        lax.all_to_all(weight_sum[None], "kv", split_axis=1, concat_axis=0, tiled=True),
        lax.all_to_all(local_peak[None], "kv", split_axis=1, concat_axis=0, tiled=True),
    )
    global_peak = jnp.max(all_peaks, axis=0)
    factor = jnp.exp(all_peaks - global_peak[None])
    merged = jnp.sum(all_parts.reshape(all_peaks.shape + (-1,)) * factor[..., None], axis=0)
    denominator = jnp.sum(all_totals * factor, axis=0)
    piece_value = (merged / denominator[..., None]).astype(jnp.bfloat16)
    decode_keys = jax.vmap(insert_row)(decode_cache, decode_rows, decode_fill)

    def attend_one(absorbed_one, turned_one, keys_one, fill_one):
        cache_places = jnp.arange(keys_one.shape[0], dtype=jnp.int32)
        return block_attend(
            absorbed_one[None], turned_one[None], keys_one, cache_places, fill_one[None], value_up
        )

    decode_part, decode_total, decode_peak = jax.vmap(attend_one)(
        decode_absorbed, decode_turned, decode_keys, decode_fill
    )
    decode_value = (decode_part[:, 0] / decode_total[:, 0, :, None]).astype(jnp.bfloat16)
    values = jnp.concatenate([piece_value, decode_value], axis=0)
    values = values.reshape(values.shape[0], -1)
    partial_value = jnp.dot(values, out_proj, preferred_element_type=jnp.float32).astype(
        jnp.bfloat16
    )
    summed = lax.psum(partial_value, "tp").astype(jnp.float32).astype(jnp.bfloat16)
    return (summed[:piece_dev], summed[piece_dev:], piece_rows, decode_rows)


def solution(mesh):
    placed = (
        P("kv", None),
        P("kv", None),
        P(),
        P("kv"),
        P("kv", None),
        P("kv", None, None),
        P(),
        P(),
        P(),
        P(None, "tp"),
        P(None, "tp"),
        P(),
        P(None, "tp"),
        P(None, "tp"),
        P("tp", None, None),
        P("tp", None, None),
        P("tp", None),
    )
    return jax.shard_map(
        local,
        mesh=mesh,
        in_specs=placed,
        out_specs=(P("kv", None), P("kv", None), P("kv", None), P("kv", None)),
        check_vma=False,
    )
```

profile of v0, /device:TPU:0, one launch (start us, length us, event | category | flops | bytes accessed | tf_op | source)
XLA Modules:
  0.0 135.7 jit_solution(8345209168863359578)
XLA Ops:
  0.7 1.3 copy.80
  3.4 0.1 fusion.14
  3.6 0.2 convolution_convert_fusion.6
  3.8 0.2 convolution_convert_fusion.5
  4.0 6.2 %all_gather.14 = bf16[5,512]{1,0:T(8,128)(2,1)S(1)} all-gather(bf16[5,128]{1,0:T(8,128)(2,1)S(1)} %convolution_convert_fusion.5), channel_id=1, replica_groups=mesh['kv'=8,'tp'=4] {'tp'}, dimensions={1}, use_global_device_ids=true | all-gather | bytes 6400 | tf_op jit(solution)/shard_map/all_gather | solution.py:122
  10.2 0.1 fusion.31
  10.3 0.3 fusion.5
  10.6 5.5 %all-gather = bf16[4,192,5]{1,2,0:T(8,128)(2,1)S(1)} all-gather(bf16[1,192,5]{1,2,0:T(8,128)(2,1)S(1)} %fusion.5), channel_id=1, replica_groups=mesh['kv'=8,'tp'=4] {'tp'}, dimensions={0}, use_global_device_ids=true | all-gather | bytes 9600 | tf_op jit(solution)/shard_map/all_gather | solution.py:121
  16.2 0.1 multiply_reduce_fusion.1
  16.4 0.2 copy.37
  16.7 0.6 copy-done.12
  17.3 0.1 fusion.48
  17.6 31.4 %all-gather.2 = bf16[8,4,544]{2,1,0:T(4,128)(2,1)S(1)} all-gather(bf16[1,4,544]{2,1,0:T(4,128)(2,1)S(1)} %slice_bitcast_fusion.14), channel_id=1, replica_groups=mesh['kv'=8,'tp'=4] {'kv'}, dimensions={0}, use_global_device_ids=true | all-gather | bytes 39168 | tf_op jit(solution)/shard_map/all_gather | solution.py:136
  49.0 0.1 multiply_cosine_fusion
  49.2 30.8 %all-gather.1 = bf16[8,4,768]{2,1,0:T(4,128)(2,1)S(1)} all-gather(bf16[1,4,768]{2,1,0:T(4,128)(2,1)S(1)} %slice_bitcast_fusion.10), channel_id=1, replica_groups=mesh['kv'=8,'tp'=4] {'kv'}, dimensions={0}, use_global_device_ids=true | all-gather | bytes 55296 | tf_op jit(solution)/shard_map/all_gather | solution.py:135
  80.0 0.1 convolution_convert_fusion.3
  80.2 0.1 reshape.414
  80.3 0.1 fusion.73
  80.4 0.2 convolution_convert_fusion.2
  80.6 0.1 reshape.413
  80.9 0.9 fusion.10
  81.7 0.2 fusion.22
  81.9 0.7 copy-done.2
  82.7 0.4 fusion.76
  83.0 0.2 fusion.12
  83.2 0.7 copy.46
  83.9 5.4 %all-to-all-start.2 = ((f32[1,32,4]{2,0,1:T(1,128)}), f32[1,32,4]{2,0,1:T(1,128)S(1)}, u32[]{:S(2)}, u32[]{:S(2)}) async-start(f32[1,32,4]{2,0,1:T(1,128)} %copy.46), calls=%async_computation.2 | async-start | bytes 32768 | tf_op jit(solution)/shard_map/all_to_all | solution.py:158
  89.4 0.1 fusion.58
  89.5 0.2 fusion.6
  89.7 0.2 fusion.11
  89.9 0.6 copy-done.14
  90.7 0.6 fusion.74
  91.3 0.8 constant_dynamic-slice_fusion
  92.0 0.1 copy.62
  92.1 0.7 copy-done.13
  92.8 2.0 %and_reduce_fusion = pred[]{:T(512)} fusion(s32[3]{0:T(128)S(1)} %copy-done.13, s32[1]{0:T(128)} %bitcast.20, s32[1]{0:T(128)} %bitcast.19, s32[1]{0:T(128)} %constant.79.clone.1), kind=kLoop, calls=%fused_computation.108 | loop fusion | flops 17 | bytes 25 | tf_op jit(solution)/shard_map/reduce.1
  94.8 1.2 broadcast_select_fusion
  96.0 0.2 copy.50
  96.2 1.6 %scatter.4 = bf16[1,768,544]{1,2,0:T(8,128)(2,1)S(1)} dynamic-update-slice(bf16[1,768,544]{1,2,0:T(8,128)(2,1)S(1)} %copy.80, bf16[1,1,544]{1,2,0:T(8,128)(2,1)S(1)} %copy.50, s32[]{:T(128)} %constant.75.clone.1, s32[]{:T(128)} %bitcast.22, s32[]{:T(128)} %constant.75.clone.1) | dynamic-update-slice | bytes 2180 | tf_op jit(solution)/shard_map/vmap(vmap())/scatter | solution.py:84
  97.9 0.1 fusion.79
  98.2 0.2 fusion.7
  98.5 0.3 fusion.75
  98.8 0.3 convolution_bitcast_fusion.1
  99.1 0.6 copy-done.7
  99.8 0.3 fusion.35
  100.1 0.3 convolution_bitcast_fusion
  100.4 0.2 fusion.37
  100.6 0.7 copy.43
  101.3 6.0 %all-to-all-start.1 = ((f32[1,32,4]{2,0,1:T(1,128)}), f32[1,32,4]{2,0,1:T(1,128)S(1)}, u32[]{:S(2)}, u32[]{:S(2)}) async-start(f32[1,32,4]{2,0,1:T(1,128)} %copy.43), calls=%async_computation.1 | async-start | bytes 32768 | tf_op jit(solution)/shard_map/all_to_all | solution.py:159
  107.4 0.6 slice.96
  108.1 0.7 reshape.442
  108.8 0.1 copy.58
  109.0 4.9 %all-to-all-done.1 = f32[1,32,4]{2,0,1:T(1,128)S(1)} async-done(((f32[1,32,4]{2,0,1:T(1,128)}), f32[1,32,4]{2,0,1:T(1,128)S(1)}, u32[]{:S(2)}, u32[]{:S(2)}) %all-to-all-start.1) | async-done | bytes 544 | tf_op jit(solution)/shard_map/all_to_all | solution.py:159
  113.9 3.3 %all-to-all-start = ((f32[1,32,256]{2,0,1:T(1,128)}), f32[1,32,256]{2,0,1:T(1,128)S(1)}, u32[]{:S(2)}, u32[]{:S(2)}) async-start(f32[1,32,256]{2,0,1:T(1,128)} %reshape.442), calls=%async_computation | async-start | bytes 65536 | tf_op jit(solution)/shard_map/all_to_all | solution.py:155
  117.2 0.1 copy.57
  117.4 0.1 copy.59
  117.5 0.1 copy.45
  117.8 0.1 mul.259
  117.9 0.1 copy.48
  118.1 5.7 %all-to-all-done = f32[1,32,256]{2,0,1:T(1,128)S(1)} async-done(((f32[1,32,256]{2,0,1:T(1,128)}), f32[1,32,256]{2,0,1:T(1,128)S(1)}, u32[]{:S(2)}, u32[]{:S(2)}) %all-to-all-start) | async-done | bytes 32800 | tf_op jit(solution)/shard_map/all_to_all | solution.py:155
  123.9 0.2 convolution_convert_fusion
  124.2 10.3 %psum.7 = bf16[5,2048]{1,0:T(8,128)(2,1)S(1)} all-reduce(bf16[5,2048]{1,0:T(8,128)(2,1)S(1)} %convolution_convert_fusion), channel_id=1, replica_groups=mesh['kv'=8,'tp'=4] {'tp'}, use_global_device_ids=true, to_apply=%region_11.12 | all-reduce | flops 10240 | bytes 40960 | tf_op jit(solution)/shard_map/psum | solution.py:183
  134.5 0.6 slice.104
  135.1 0.6 slice.105
  (67 shorter events, 1.7 us)
Async XLA Ops:
  0.6 123.3 %copy-start = (bf16[256,2048]{1,0:T(8,128)(2,1)S(1)}, bf16[256,2048]{1,0:T(8,128)(2,1)}, u32[]{:S(2)}) copy-start(bf16[256,2048]{1,0:T(8,128)(2,1)} %param.35) | copy-start | bytes 3145732
  0.6 3.1 %copy-start.5 = (bf16[2048,128]{1,0:T(8,128)(2,1)S(1)}, bf16[2048,128]{1,0:T(8,128)(2,1)}, u32[]{:S(2)}) copy-start(bf16[2048,128]{1,0:T(8,128)(2,1)} %param.29) | copy-start | bytes 1572868
  0.7 2.9 %copy-start.15 = (bf16[2048,32]{0,1:T(8,128)(2,1)S(1)}, bf16[2048,32]{0,1:T(8,128)(2,1)}, u32[]{:S(2)}) copy-start(bf16[2048,32]{0,1:T(8,128)(2,1)} %param.30) | copy-start | bytes 393220
  0.7 2.7 %copy-start.8 = (bf16[4,2048]{1,0:T(4,128)(2,1)S(1)}, bf16[4,2048]{1,0:T(4,128)(2,1)}, u32[]{:S(2)}) copy-start(bf16[4,2048]{1,0:T(4,128)(2,1)} %param.19) | copy-start | bytes 49156
  0.7 2.7 %copy-start.9 = (bf16[1,2048]{1,0:T(2,128)(2,1)S(1)}, bf16[1,2048]{1,0:T(2,128)(2,1)}, u32[]{:S(2)}) copy-start(bf16[1,2048]{1,0:T(2,128)(2,1)} %param.20) | copy-start | bytes 12292
  0.7 2.9 %copy-start.10 = (f32[2048]{0:T(1024)S(1)}, f32[2048]{0:T(1024)}, u32[]{:S(2)}) copy-start(f32[2048]{0:T(1024)} %param.25) | copy-start | bytes 24580
  2.0 8.3 %copy-start.3 = (bf16[2048,192]{0,1:T(8,128)(2,1)S(1)}, bf16[2048,192]{0,1:T(8,128)(2,1)}, u32[]{:S(2)}) copy-start(bf16[2048,192]{0,1:T(8,128)(2,1)} %param.28) | copy-start | bytes 2359300
  10.3 6.1 %copy-start.6 = (bf16[256,544]{0,1:T(8,128)(2,1)S(1)}, bf16[256,544]{0,1:T(8,128)(2,1)}, u32[]{:S(2)}) copy-start(bf16[256,544]{0,1:T(8,128)(2,1)} %param.23) | copy-start | bytes 835588
  16.6 0.7 copy-start.12
  17.3 31.8 %copy-start.11 = (f32[768]{0:T(1024)S(1)}, f32[768]{0:T(1024)}, u32[]{:S(2)}) copy-start(f32[768]{0:T(1024)} %param.26) | copy-start | bytes 9220
  17.5 62.5 %copy-start.4 = (bf16[768,128]{1,0:T(8,128)(2,1)S(1)}, bf16[768,128]{1,0:T(8,128)(2,1)}, u32[]{:S(2)}) copy-start(bf16[768,128]{1,0:T(8,128)(2,1)} %param.32) | copy-start | bytes 589828
  17.5 62.8 %copy-start.1 = (bf16[768,256]{1,0:T(8,128)(2,1)S(1)}, bf16[768,256]{1,0:T(8,128)(2,1)}, u32[]{:S(2)}) copy-start(bf16[768,256]{1,0:T(8,128)(2,1)} %param.31) | copy-start | bytes 1179652
  81.7 1.0 copy-start.2
  83.9 17.4 %all-to-all-start.2 = ((f32[1,32,4]{2,0,1:T(1,128)}), f32[1,32,4]{2,0,1:T(1,128)S(1)}, u32[]{:S(2)}, u32[]{:S(2)}) async-start(f32[1,32,4]{2,0,1:T(1,128)} %copy.46), calls=%async_computation.2 | async-start | bytes 32768 | tf_op jit(solution)/shard_map/all_to_all | solution.py:158
  89.9 0.7 copy-start.14
  92.1 0.7 copy-start.13
  98.8 1.0 copy-start.7
  101.3 12.6 %all-to-all-start.1 = ((f32[1,32,4]{2,0,1:T(1,128)}), f32[1,32,4]{2,0,1:T(1,128)S(1)}, u32[]{:S(2)}, u32[]{:S(2)}) async-start(f32[1,32,4]{2,0,1:T(1,128)} %copy.43), calls=%async_computation.1 | async-start | bytes 32768 | tf_op jit(solution)/shard_map/all_to_all | solution.py:159
  113.9 10.0 %all-to-all-start = ((f32[1,32,256]{2,0,1:T(1,128)}), f32[1,32,256]{2,0,1:T(1,128)S(1)}, u32[]{:S(2)}, u32[]{:S(2)}) async-start(f32[1,32,256]{2,0,1:T(1,128)} %reshape.442), calls=%async_computation | async-start | bytes 65536 | tf_op jit(solution)/shard_map/all_to_all | solution.py:155
where the time goes:
time: 136 us
  blocking collectives  84.1 us (62%)
  starting transfers between devices  14.8 us (11%)
  local copies, waits for them, and re-layouts  13.7 us (10%)
  waiting for transfers between devices  10.7 us (8%)
  other arithmetic  5.93 us (4%)
  matrix products  4.06 us (3%)
  between operations  2.43 us (2%)
    all_gather x1, blocking collectives, local(): lax.all_gather(piece_rows, 'kv', axis=0, tiled=True)  31.4 us
    all_gather x1, blocking collectives, local(): lax.all_gather(query_lat[:piece_dev], 'kv', axis=0, tiled=True)  30.8 us
    psum x1, blocking collectives, local(): lax.psum(partial_value, 'tp').astype(jnp.float32).astype(jnp.bfloat16)  10.3 us
    all_gather x1, blocking collectives, local(): lax.all_gather(latent_comp, 'tp', axis=1, tiled=True)  6.16 us
    all_to_all x1, starting transfers between devices, local(): lax.all_to_all(local_peak[None], 'kv', split_axis=1, concat_axis=0, tiled...  6 us
    all_to_all x1, waiting for transfers between devices, local(): lax.all_to_all(partial_sum.reshape(1, piece_total, -1), 'kv', split_axis=...  5.73 us
    all_gather x1, blocking collectives, local(): lax.all_gather(query_comp, 'tp', axis=1, tiled=True)  5.5 us
    all_to_all x1, starting transfers between devices, local(): lax.all_to_all(weight_sum[None], 'kv', split_axis=1, concat_axis=0, tiled...  5.43 us
  transfers between devices with their start and end apart: 3, of which 2 were waited for; matrix products, arithmetic and copies ran while one was open for 9% of the time, Pallas kernels for 0%

commit v1 on v0

--- a/solution.py
+++ b/solution.py
@@ -180,7 +180,11 @@
     partial_value = jnp.dot(values, out_proj, preferred_element_type=jnp.float32).astype(
         jnp.bfloat16
     )
-    summed = lax.psum(partial_value, "tp").astype(jnp.float32).astype(jnp.bfloat16)
+    summed = (
+        jnp.sum(lax.all_gather(partial_value, "tp"), axis=0)
+        .astype(jnp.float32)
+        .astype(jnp.bfloat16)
+    )
     return (summed[:piece_dev], summed[piece_dev:], piece_rows, decode_rows)
 
 

time: 136 us -> 131 us (0.963)
  blocking collectives: 84.1 us -> 79.2 us
    psum x1 -> x0, blocking collectives: 10.3 us -> none  [local(): lax.psum(partial_value, 'tp').astype(jnp.float32).astype(jnp.bfloat16)]
    all_gather x0 -> x1, blocking collectives: none -> 5.41 us  [local(): lax.all_gather(partial_value, 'tp')]
where the time goes in v1:
time: 131 us
  blocking collectives  79.2 us (60%)
  starting transfers between devices  14.8 us (11%)
  local copies, waits for them, and re-layouts  13.7 us (10%)
  waiting for transfers between devices  10.7 us (8%)
  other arithmetic  5.96 us (5%)
  matrix products  4.06 us (3%)
  between operations  2.43 us (2%)
    all_gather x1, blocking collectives, local(): lax.all_gather(piece_rows, 'kv', axis=0, tiled=True)  31.4 us
    all_gather x1, blocking collectives, local(): lax.all_gather(query_lat[:piece_dev], 'kv', axis=0, tiled=True)  30.8 us
    all_gather x1, blocking collectives, local(): lax.all_gather(latent_comp, 'tp', axis=1, tiled=True)  6.16 us
    all_to_all x1, starting transfers between devices, local(): lax.all_to_all(local_peak[None], 'kv', split_axis=1, concat_axis=0, tiled...  6 us
    all_to_all x1, waiting for transfers between devices, local(): lax.all_to_all(partial_sum.reshape(1, piece_total, -1), 'kv', split_axis=...  5.73 us
    all_gather x1, blocking collectives, local(): lax.all_gather(query_comp, 'tp', axis=1, tiled=True)  5.5 us
    all_to_all x1, starting transfers between devices, local(): lax.all_to_all(weight_sum[None], 'kv', split_axis=1, concat_axis=0, tiled...  5.43 us
    all_gather x1, blocking collectives, local(): lax.all_gather(partial_value, 'tp')  5.41 us
  transfers between devices with their start and end apart: 3, of which 2 were waited for; matrix products, arithmetic and copies ran while one was open for 9% of the time, Pallas kernels for 0%

profile of v1, /device:TPU:0, one launch (start us, length us, event | category | flops | bytes accessed | tf_op | source)
XLA Modules:
  0.0 130.9 jit_solution(18031131417268661305)
XLA Ops:
  0.7 1.3 copy.80
  3.4 0.1 fusion.15
  3.6 0.2 convolution_convert_fusion.6
  3.8 0.2 convolution_convert_fusion.5
  4.0 6.2 %all_gather.20 = bf16[5,512]{1,0:T(8,128)(2,1)S(1)} all-gather(bf16[5,128]{1,0:T(8,128)(2,1)S(1)} %convolution_convert_fusion.5), channel_id=1, replica_groups=mesh['kv'=8,'tp'=4] {'tp'}, dimensions={1}, use_global_device_ids=true | all-gather | bytes 6400 | tf_op jit(solution)/shard_map/all_gather | solution.py:122
  10.2 0.1 fusion.32
  10.3 0.3 fusion.6
  10.6 5.5 %all-gather.1 = bf16[4,192,5]{1,2,0:T(8,128)(2,1)S(1)} all-gather(bf16[1,192,5]{1,2,0:T(8,128)(2,1)S(1)} %fusion.6), channel_id=1, replica_groups=mesh['kv'=8,'tp'=4] {'tp'}, dimensions={0}, use_global_device_ids=true | all-gather | bytes 9600 | tf_op jit(solution)/shard_map/all_gather | solution.py:121
  16.2 0.1 multiply_reduce_fusion.1
  16.4 0.2 copy.37
  16.7 0.6 copy-done.12
  17.3 0.1 fusion.49
  17.6 31.4 %all-gather.3 = bf16[8,4,544]{2,1,0:T(4,128)(2,1)S(1)} all-gather(bf16[1,4,544]{2,1,0:T(4,128)(2,1)S(1)} %slice_bitcast_fusion.14), channel_id=1, replica_groups=mesh['kv'=8,'tp'=4] {'kv'}, dimensions={0}, use_global_device_ids=true | all-gather | bytes 39168 | tf_op jit(solution)/shard_map/all_gather | solution.py:136
  49.0 0.1 multiply_cosine_fusion
  49.2 30.8 %all-gather.2 = bf16[8,4,768]{2,1,0:T(4,128)(2,1)S(1)} all-gather(bf16[1,4,768]{2,1,0:T(4,128)(2,1)S(1)} %slice_bitcast_fusion.10), channel_id=1, replica_groups=mesh['kv'=8,'tp'=4] {'kv'}, dimensions={0}, use_global_device_ids=true | all-gather | bytes 55296 | tf_op jit(solution)/shard_map/all_gather | solution.py:135
  80.0 0.1 convolution_convert_fusion.3
  80.2 0.1 reshape.414
  80.3 0.1 fusion.74
  80.4 0.2 convolution_convert_fusion.2
  80.6 0.1 reshape.413
  80.9 0.9 fusion.11
  81.7 0.2 fusion.23
  81.9 0.7 copy-done.2
  82.7 0.4 fusion.77
  83.0 0.2 fusion.13
  83.2 0.7 copy.46
  83.9 5.4 %all-to-all-start.2 = ((f32[1,32,4]{2,0,1:T(1,128)}), f32[1,32,4]{2,0,1:T(1,128)S(1)}, u32[]{:S(2)}, u32[]{:S(2)}) async-start(f32[1,32,4]{2,0,1:T(1,128)} %copy.46), calls=%async_computation.2 | async-start | bytes 32768 | tf_op jit(solution)/shard_map/all_to_all | solution.py:158
  89.4 0.1 fusion.59
  89.5 0.2 fusion.7
  89.7 0.2 fusion.12
  89.9 0.6 copy-done.14
  90.7 0.6 fusion.75
  91.3 0.8 constant_dynamic-slice_fusion
  92.0 0.1 copy.62
  92.1 0.7 copy-done.13
  92.8 2.0 %and_reduce_fusion = pred[]{:T(512)} fusion(s32[3]{0:T(128)S(1)} %copy-done.13, s32[1]{0:T(128)} %bitcast.20, s32[1]{0:T(128)} %bitcast.19, s32[1]{0:T(128)} %constant.80.clone.1), kind=kLoop, calls=%fused_computation.109 | loop fusion | flops 17 | bytes 25 | tf_op jit(solution)/shard_map/reduce.1
  94.8 1.2 broadcast_select_fusion
  96.0 0.2 copy.50
  96.2 1.6 %scatter.4 = bf16[1,768,544]{1,2,0:T(8,128)(2,1)S(1)} dynamic-update-slice(bf16[1,768,544]{1,2,0:T(8,128)(2,1)S(1)} %copy.80, bf16[1,1,544]{1,2,0:T(8,128)(2,1)S(1)} %copy.50, s32[]{:T(128)} %constant.76.clone.1, s32[]{:T(128)} %bitcast.22, s32[]{:T(128)} %constant.76.clone.1) | dynamic-update-slice | bytes 2180 | tf_op jit(solution)/shard_map/vmap(vmap())/scatter | solution.py:84
  97.9 0.1 fusion.80
  98.2 0.2 fusion.8
  98.5 0.3 fusion.76
  98.8 0.3 convolution_bitcast_fusion.1
  99.1 0.6 copy-done.7
  99.8 0.3 fusion.36
  100.1 0.3 convolution_bitcast_fusion
  100.4 0.2 fusion.38
  100.6 0.7 copy.43
  101.3 6.0 %all-to-all-start.1 = ((f32[1,32,4]{2,0,1:T(1,128)}), f32[1,32,4]{2,0,1:T(1,128)S(1)}, u32[]{:S(2)}, u32[]{:S(2)}) async-start(f32[1,32,4]{2,0,1:T(1,128)} %copy.43), calls=%async_computation.1 | async-start | bytes 32768 | tf_op jit(solution)/shard_map/all_to_all | solution.py:159
  107.4 0.6 slice.96
  108.1 0.7 reshape.446
  108.8 0.1 copy.58
  109.0 4.9 %all-to-all-done.1 = f32[1,32,4]{2,0,1:T(1,128)S(1)} async-done(((f32[1,32,4]{2,0,1:T(1,128)}), f32[1,32,4]{2,0,1:T(1,128)S(1)}, u32[]{:S(2)}, u32[]{:S(2)}) %all-to-all-start.1) | async-done | bytes 544 | tf_op jit(solution)/shard_map/all_to_all | solution.py:159
  113.9 3.3 %all-to-all-start = ((f32[1,32,256]{2,0,1:T(1,128)}), f32[1,32,256]{2,0,1:T(1,128)S(1)}, u32[]{:S(2)}, u32[]{:S(2)}) async-start(f32[1,32,256]{2,0,1:T(1,128)} %reshape.446), calls=%async_computation | async-start | bytes 65536 | tf_op jit(solution)/shard_map/all_to_all | solution.py:155
  117.2 0.1 copy.57
  117.4 0.1 copy.59
  117.5 0.1 copy.45
  117.8 0.1 mul.259
  117.9 0.1 copy.48
  118.1 5.7 %all-to-all-done = f32[1,32,256]{2,0,1:T(1,128)S(1)} async-done(((f32[1,32,256]{2,0,1:T(1,128)}), f32[1,32,256]{2,0,1:T(1,128)S(1)}, u32[]{:S(2)}, u32[]{:S(2)}) %all-to-all-start) | async-done | bytes 32800 | tf_op jit(solution)/shard_map/all_to_all | solution.py:155
  123.9 0.2 fusion
  124.2 5.4 %all-gather.4 = bf16[4,5,2048]{2,1,0:T(8,128)(2,1)S(1)} all-gather(bf16[1,5,2048]{2,1,0:T(8,128)(2,1)S(1)} %fusion), channel_id=2, replica_groups=mesh['kv'=8,'tp'=4] {'tp'}, dimensions={0}, use_global_device_ids=true | all-gather | bytes 102400 | tf_op jit(solution)/shard_map/all_gather | solution.py:184
  129.6 0.6 slice.104
  130.2 0.6 slice.105
  (68 shorter events, 1.7 us)
Async XLA Ops:
  0.6 123.3 %copy-start = (bf16[256,2048]{1,0:T(8,128)(2,1)S(1)}, bf16[256,2048]{1,0:T(8,128)(2,1)}, u32[]{:S(2)}) copy-start(bf16[256,2048]{1,0:T(8,128)(2,1)} %param.35) | copy-start | bytes 3145732
  0.6 3.1 %copy-start.5 = (bf16[2048,128]{1,0:T(8,128)(2,1)S(1)}, bf16[2048,128]{1,0:T(8,128)(2,1)}, u32[]{:S(2)}) copy-start(bf16[2048,128]{1,0:T(8,128)(2,1)} %param.29) | copy-start | bytes 1572868
  0.7 2.9 %copy-start.15 = (bf16[2048,32]{0,1:T(8,128)(2,1)S(1)}, bf16[2048,32]{0,1:T(8,128)(2,1)}, u32[]{:S(2)}) copy-start(bf16[2048,32]{0,1:T(8,128)(2,1)} %param.30) | copy-start | bytes 393220
  0.7 2.7 %copy-start.8 = (bf16[4,2048]{1,0:T(4,128)(2,1)S(1)}, bf16[4,2048]{1,0:T(4,128)(2,1)}, u32[]{:S(2)}) copy-start(bf16[4,2048]{1,0:T(4,128)(2,1)} %param.19) | copy-start | bytes 49156
  0.7 2.7 %copy-start.9 = (bf16[1,2048]{1,0:T(2,128)(2,1)S(1)}, bf16[1,2048]{1,0:T(2,128)(2,1)}, u32[]{:S(2)}) copy-start(bf16[1,2048]{1,0:T(2,128)(2,1)} %param.20) | copy-start | bytes 12292
  0.7 2.9 %copy-start.10 = (f32[2048]{0:T(1024)S(1)}, f32[2048]{0:T(1024)}, u32[]{:S(2)}) copy-start(f32[2048]{0:T(1024)} %param.25) | copy-start | bytes 24580
  2.0 8.3 %copy-start.3 = (bf16[2048,192]{0,1:T(8,128)(2,1)S(1)}, bf16[2048,192]{0,1:T(8,128)(2,1)}, u32[]{:S(2)}) copy-start(bf16[2048,192]{0,1:T(8,128)(2,1)} %param.28) | copy-start | bytes 2359300
  10.3 6.1 %copy-start.6 = (bf16[256,544]{0,1:T(8,128)(2,1)S(1)}, bf16[256,544]{0,1:T(8,128)(2,1)}, u32[]{:S(2)}) copy-start(bf16[256,544]{0,1:T(8,128)(2,1)} %param.23) | copy-start | bytes 835588
  16.6 0.7 copy-start.12
  17.3 31.8 %copy-start.11 = (f32[768]{0:T(1024)S(1)}, f32[768]{0:T(1024)}, u32[]{:S(2)}) copy-start(f32[768]{0:T(1024)} %param.26) | copy-start | bytes 9220
  17.5 62.5 %copy-start.4 = (bf16[768,128]{1,0:T(8,128)(2,1)S(1)}, bf16[768,128]{1,0:T(8,128)(2,1)}, u32[]{:S(2)}) copy-start(bf16[768,128]{1,0:T(8,128)(2,1)} %param.32) | copy-start | bytes 589828
  17.5 62.8 %copy-start.1 = (bf16[768,256]{1,0:T(8,128)(2,1)S(1)}, bf16[768,256]{1,0:T(8,128)(2,1)}, u32[]{:S(2)}) copy-start(bf16[768,256]{1,0:T(8,128)(2,1)} %param.31) | copy-start | bytes 1179652
  81.7 1.0 copy-start.2
  83.9 17.4 %all-to-all-start.2 = ((f32[1,32,4]{2,0,1:T(1,128)}), f32[1,32,4]{2,0,1:T(1,128)S(1)}, u32[]{:S(2)}, u32[]{:S(2)}) async-start(f32[1,32,4]{2,0,1:T(1,128)} %copy.46), calls=%async_computation.2 | async-start | bytes 32768 | tf_op jit(solution)/shard_map/all_to_all | solution.py:158
  89.9 0.7 copy-start.14
  92.1 0.7 copy-start.13
  98.8 1.0 copy-start.7
  101.3 12.6 %all-to-all-start.1 = ((f32[1,32,4]{2,0,1:T(1,128)}), f32[1,32,4]{2,0,1:T(1,128)S(1)}, u32[]{:S(2)}, u32[]{:S(2)}) async-start(f32[1,32,4]{2,0,1:T(1,128)} %copy.43), calls=%async_computation.1 | async-start | bytes 32768 | tf_op jit(solution)/shard_map/all_to_all | solution.py:159
  113.9 10.0 %all-to-all-start = ((f32[1,32,256]{2,0,1:T(1,128)}), f32[1,32,256]{2,0,1:T(1,128)S(1)}, u32[]{:S(2)}, u32[]{:S(2)}) async-start(f32[1,32,256]{2,0,1:T(1,128)} %reshape.446), calls=%async_computation | async-start | bytes 65536 | tf_op jit(solution)/shard_map/all_to_all | solution.py:155
